TPU v7x, 128 devices: a whole 4x4x4 slice. The times are simulated.
128 devices in a mesh: ep: 32 (over z, y, core), tp: 4 (over x).
Axes of the slice: x: 4, y: 4, z: 4, core: 2. Of those that a mesh axis runs over, the one named last changes fastest.
Arguments:
- q_latent: bfloat16 [16384, 512], P(('ep', 'tp')), may hold values from -6 to 6
- kv_latent: bfloat16 [16384, 256], P(('ep', 'tp')), may hold values from -6 to 6
- rope_key: bfloat16 [16384, 32], P(('ep', 'tp')), may hold values from -240 to 240
- q_gain: float32 [512], replicated, may hold values from 0.1 to 1.9
- kv_gain: float32 [256], replicated, may hold values from 0.1 to 1.9
- w_query: bfloat16 [512, 1024], P(None, 'tp'), may hold values from -0.25 to 0.25
- w_query_rot: bfloat16 [512, 512], P(None, 'tp'), may hold values from -0.25 to 0.25
- w_key: bfloat16 [256, 1024], P(None, 'tp'), may hold values from -0.375 to 0.375
- w_value: bfloat16 [256, 1024], P(None, 'tp'), may hold values from -0.375 to 0.375
- w_mix_out: bfloat16 [1024, 2048], P('tp'), may hold values from -0.1875 to 0.1875
- expert_input: bfloat16 [16384, 2048], P(('ep', 'tp')), may hold values from -6 to 6
- ffn_gain: float32 [2048], replicated, may hold values from 0.1 to 1.9
- expert_ids: int32 [16384, 4], P(('ep', 'tp')), may hold values from 0 to 31, all different within a row; in each aligned block of 128 rows (0 to 127, 128 to 255, ...) at most 24 rows name the same one
- route_weights: float32 [16384, 4], P(('ep', 'tp')), may hold values from 0.2 to 1
- w_gate_exp: bfloat16 [32, 2048, 1024], P('ep', None, 'tp'), may hold values from -0.125 to 0.125
- w_up_exp: bfloat16 [32, 2048, 1024], P('ep', None, 'tp'), may hold values from -0.125 to 0.125
- w_down_exp: bfloat16 [32, 1024, 2048], P('ep', 'tp'), may hold values from -0.1875 to 0.1875
Outputs:
- mixer_out: bfloat16 [16384, 2048], P(('ep', 'tp'))
- expert_out: bfloat16 [16384, 2048], P(('ep', 'tp'))
Inputs may be any that keep to these rules, and one draw needn't show every extreme that they name: `expert_ids`: the experts of a row are all different. In the rows of one device (aligned blocks of 128 tokens) no expert is named by more than 24 rows, a bound that some block reaches.
All inputs are finite; a program needn't handle non-finite values.
Results may differ from a plain program's by a relative error of at most 0.012.
The roundings to bfloat16 on the way count: a program that leaves them out, or rounds other values in their place, can miss the bound.
Values may be sent and summed in bfloat16 or wider, within the bound.
A program may use at most 128 MiB of HBM per device.

v0:
```python
import jax
import jax.numpy as jnp
from jax import lax
from jax.sharding import PartitionSpec as P

D = 2048
NOPE = 64
ROPE = 32
VD = 64
TOPK = 4
SEG = 64
norm_epsilon = 1e-06
rope_base = 10000.0
masked_score = -1e30


def rms_scale(values_in, gain_vec):
    floats = values_in.astype(jnp.float32)
    return (
        floats
        * lax.rsqrt(jnp.mean(floats * floats, axis=-1, keepdims=True) + norm_epsilon)
        * gain_vec
    )


def tables(positions):
    half_width = ROPE // 2
    frequency = rope_base ** (-jnp.arange(half_width, dtype=jnp.float32) / half_width)
    angles = positions.astype(jnp.float32)[:, None] * frequency[None, :]
    return (jnp.cos(angles), jnp.sin(angles))


def rotate_pairs(values_in, cosine, sine_table):
    half_width = values_in.shape[-1] // 2
    first, second = (values_in[..., :half_width], values_in[..., half_width:])
    return jnp.concatenate(
        [first * cosine - second * sine_table, first * sine_table + second * cosine], axis=-1
    )


def on_device(
    q_latent,
    kv_latent,
    rope_key,
    q_gain,
    kv_gain,
    w_query,
    w_query_rot,
    w_key,
    w_value,
    w_mix_out,
    expert_input,
    ffn_gain,
    expert_ids,
    route_weights,
    w_gate_exp,
    w_up_exp,
    w_down_exp,
):
    tok_rows = q_latent.shape[0]
    tp_count = lax.axis_size("tp")
    group_rows = tp_count * tok_rows
    group_start = lax.axis_index("ep") * group_rows
    heads_here = w_key.shape[1] // NOPE
    score_scale = (NOPE + ROPE) ** (-0.5)
    shard_rows = lax.all_gather(q_latent, "tp", axis=0, tiled=True)
    row_count = shard_rows.shape[0]
    positions = group_start + jnp.arange(row_count, dtype=jnp.int32)
    cosine, sine_table = tables(positions)
    normed = rms_scale(shard_rows, q_gain).astype(jnp.bfloat16)
    plain = jnp.dot(normed, w_query, preferred_element_type=jnp.float32).astype(jnp.bfloat16)
    turned = jnp.dot(normed, w_query_rot, preferred_element_type=jnp.float32).reshape(
        row_count, heads_here, ROPE
    )
    turned = rotate_pairs(turned, cosine[:, None, :], sine_table[:, None, :]).astype(jnp.bfloat16)
    queries = jnp.concatenate([plain, turned.reshape(row_count, heads_here * ROPE)], axis=1)
    q_plain = queries[:, : heads_here * NOPE].reshape(group_rows, heads_here, NOPE)
    q_turned = queries[:, heads_here * NOPE :].reshape(group_rows, heads_here, ROPE)
    query_segment = (group_start + jnp.arange(group_rows, dtype=jnp.int32)) // SEG
    last_segment = (group_start + group_rows - 1) // SEG
    start_state = (
        jnp.full((heads_here, group_rows), masked_score, jnp.float32),
        jnp.zeros((heads_here, group_rows), jnp.float32),
        jnp.zeros((heads_here, group_rows, VD), jnp.float32),
    )
    first_row = jnp.int32(0)
    latents = lax.all_gather(kv_latent, ("ep", "tp"), axis=0, tiled=True)
    rope_rows = lax.all_gather(rope_key, ("ep", "tp"), axis=0, tiled=True)
    shard_count = latents.shape[0] // tok_rows
    grouping = 1
    for divisor in range(1, shard_count + 1):
        if shard_count % divisor == 0 and divisor * tok_rows <= max(512, tok_rows):
            grouping = divisor
    key_rows = grouping * tok_rows

    def key_work(state, offset):
        run_max, weight_sum, weighted = state
        latent_block = lax.dynamic_slice_in_dim(latents, offset, key_rows, 0)
        rope_block = lax.dynamic_slice_in_dim(rope_rows, offset, key_rows, 0)
        positions = first_row + offset + jnp.arange(key_rows, dtype=jnp.int32)
        cosine, sine_table = tables(positions)
        normed = rms_scale(latent_block, kv_gain).astype(jnp.bfloat16)
        k_plain = jnp.dot(normed, w_key, preferred_element_type=jnp.float32).astype(jnp.bfloat16)
        k_plain = k_plain.reshape(key_rows, heads_here, NOPE)
        values = jnp.dot(normed, w_value, preferred_element_type=jnp.float32).astype(jnp.bfloat16)
        values = values.reshape(key_rows, heads_here, VD)
        k_turned = rotate_pairs(rope_block.astype(jnp.float32), cosine, sine_table).astype(
            jnp.bfloat16
        )
        scores = jnp.einsum("qhd,khd->hqk", q_plain, k_plain, preferred_element_type=jnp.float32)
        scores = scores + jnp.einsum(
            "qhd,kd->hqk", q_turned, k_turned, preferred_element_type=jnp.float32
        )
        scores = scores * score_scale
        allowed = (positions // SEG)[None, :] <= query_segment[:, None]
        scores = jnp.where(allowed[None], scores, masked_score)
        new_max = jnp.maximum(run_max, jnp.max(scores, axis=-1))
        weights = jnp.where(allowed[None], jnp.exp(scores - new_max[:, :, None]), 0.0)
        factor = jnp.exp(run_max - new_max)
        weight_sum = weight_sum * factor + jnp.sum(weights, axis=-1)
        weighted = weighted * factor[:, :, None] + jnp.einsum(
            "hqk,khd->hqd", weights.astype(jnp.bfloat16), values, preferred_element_type=jnp.float32
        )
        return (new_max, weight_sum, weighted)

    def key_step(state, block_number):
        offset = block_number * key_rows
        visible = (first_row + offset) // SEG <= last_segment
        updated = lax.cond(
            visible, lambda carried: key_work(carried, offset), lambda carried: carried, state
        )
        return (updated, None)

    result_state, _ = lax.scan(
        key_step, start_state, jnp.arange(shard_count // grouping, dtype=jnp.int32)
    )
    run_max, weight_sum, weighted = result_state
    attention = (
        (weighted / weight_sum[:, :, None])
        .transpose(1, 0, 2)
        .astype(jnp.bfloat16)
        .reshape(group_rows, heads_here * VD)
    )
    chosen = attention
    partial_out = jnp.dot(chosen, w_mix_out, preferred_element_type=jnp.float32).astype(
        jnp.bfloat16
    )
    mixer_out = lax.psum_scatter(
        lax.optimization_barrier(partial_out).astype(jnp.float32).astype(jnp.bfloat16),
        "tp",
        scatter_dimension=0,
        tiled=True,
    )
    expert_count = lax.axis_size("ep")
    slot_count = 3 * tok_rows * TOPK // (2 * expert_count)
    gate_weight = w_gate_exp[0]
    up_weight = w_up_exp[0]
    down_weight = w_down_exp[0]
    normed = rms_scale(expert_input, ffn_gain).astype(jnp.bfloat16)
    routed = expert_ids.reshape(-1)
    onehot = (routed[:, None] == jnp.arange(expert_count, dtype=jnp.int32)[None, :]).astype(
        jnp.int32
    )
    slot_number = jnp.sum((jnp.cumsum(onehot, axis=0) - 1) * onehot, axis=-1)
    slot_place = (routed * slot_count + slot_number).reshape(tok_rows, TOPK)
    slot_line = jnp.arange(expert_count * slot_count, dtype=jnp.int32)
    picks = [
        (slot_place[:, route_rank][:, None] == slot_line[None, :]).astype(jnp.bfloat16)
        for route_rank in range(TOPK)
    ]
    dispatch = picks[0]
    for route_rank in range(1, TOPK):
        dispatch = dispatch + picks[route_rank]
    outgoing = lax.dot_general(
        dispatch, normed, (((0,), (0,)), ((), ())), preferred_element_type=jnp.float32
    ).astype(jnp.bfloat16)
    copies = jnp.broadcast_to(
        outgoing.reshape(expert_count, 1, slot_count, D), (expert_count, tp_count, slot_count, D)
    )
    copies = copies.reshape(expert_count * tp_count, slot_count, D)
    arrived = lax.all_to_all(copies, ("ep", "tp"), split_axis=0, concat_axis=0, tiled=True)
    sources, item_count, feature_width = arrived.shape
    chosen = arrived.reshape(sources * item_count, feature_width)
    gate_part = jnp.dot(chosen, gate_weight, preferred_element_type=jnp.float32)
    up_part = jnp.dot(chosen, up_weight, preferred_element_type=jnp.float32)
    hidden = (jax.nn.silu(gate_part) * up_part).astype(jnp.bfloat16)
    partial_out = jnp.dot(hidden, down_weight, preferred_element_type=jnp.float32).astype(
        jnp.bfloat16
    )
    returned = lax.all_to_all(
        partial_out.reshape(sources, item_count, feature_width),
        ("ep", "tp"),
        split_axis=0,
        concat_axis=0,
        tiled=True,
    )
    block_parts = returned.reshape(expert_count, tp_count, slot_count, D).astype(jnp.float32)
    results = (
        jnp.sum(block_parts, axis=1).astype(jnp.bfloat16).reshape(expert_count * slot_count, D)
    )
    combined = jnp.zeros((tok_rows, D), jnp.float32)
    for route_rank in range(TOPK):
        fetched = jnp.dot(picks[route_rank], results, preferred_element_type=jnp.float32)
        combined = combined + route_weights[:, route_rank : route_rank + 1] * fetched
    expert_out = combined.astype(jnp.bfloat16)
    return (mixer_out, expert_out)


def solution(mesh):
    return jax.shard_map(
        on_device,
        mesh=mesh,
        in_specs=(
            P(("ep", "tp"), None),
            P(("ep", "tp"), None),
            P(("ep", "tp"), None),
            P(),
            P(),
            P(None, "tp"),
            P(None, "tp"),
            P(None, "tp"),
            P(None, "tp"),
            P("tp", None),
            P(("ep", "tp"), None),
            P(),
            P(("ep", "tp"), None),
            P(("ep", "tp"), None),
            P("ep", None, "tp"),
            P("ep", None, "tp"),
            P("ep", "tp", None),
        ),
        out_specs=(P(("ep", "tp"), None), P(("ep", "tp"), None)),
        check_vma=False,
    )
```

profile of v0, /device:TPU:1, one launch (start us, length us, event | category | flops | bytes accessed | tf_op | source)
XLA Modules:
  0.0 609.9 jit_solution(8935028124554305752)
XLA Ops:
  12.1 1.2 fusion.50
  13.4 3.9 convolution_convert_fusion.3
  17.3 8.2 %broadcast_in_dim.42 = bf16[32,4,24,2048]{3,2,1,0:T(8,128)(2,1)} broadcast(bf16[32,24,2048]{2,1,0:T(8,128)(2,1)} %bitcast.95), dimensions={0,2,3} | broadcast | bytes 15728640 | tf_op jit(solution)/shard_map/broadcast_in_dim | solution.py:177
  25.5 11.9 %all-to-all-start = ((bf16[128,24,2048]{2,1,0:T(8,128)(2,1)}), bf16[128,24,2048]{2,1,0:T(8,128)(2,1)}, u32[]{:S(2)}, u32[]{:S(2)}) async-start(bf16[128,24,2048]{2,1,0:T(8,128)(2,1)} %bitcast.91), calls=%async_computation.1 | async-start | bytes 25165824 | tf_op jit(solution)/shard_map/all_to_all | solution.py:181
  37.4 156.9 %all_gather.10 = bf16[512,512]{1,0:T(8,128)(2,1)S(1)} all-gather(bf16[128,512]{1,0:T(8,128)(2,1)S(1)} %copy-done.6), channel_id=1, replica_groups=mesh['ep'=32,'tp'=4] {'tp'}, dimensions={0}, use_global_device_ids=true | all-gather | bytes 655360 | tf_op jit(solution)/shard_map/all_gather | solution.py:66
  196.9 9.7 %fusion.56 = f32[3072,256]{1,0:T(8,128)} fusion(bf16[3072,2048]{1,0:T(8,128)(2,1)} %bitcast.17, bf16[1,2048,256]{2,1,0:T(8,128)(2,1)S(1)} %copy-done.9), kind=kOutput, calls=%fused_computation.90 | convolution fusion | flops 3221225472 | bytes 16777216 | tf_op jit(solution)/shard_map/dot_general | solution.py:184
  206.5 19.1 %convolution_convert_fusion.2 = bf16[3072,2048]{1,0:T(8,128)(2,1)} fusion(bf16[3072,2048]{1,0:T(8,128)(2,1)} %bitcast.17, f32[3072,256]{1,0:T(8,128)} %fusion.56, bf16[1,256,2048]{2,1,0:T(8,128)(2,1)S(1)} %copy-done, bf16[1,2048,256]{2,1,0:T(8,128)(2,1)} %param.36), kind=kOutput, calls=%fused_computation.63 | convolution fusion | flops 6453460992 | bytes 30408704 | tf_op jit(solution)/shard_map/dot_general | solution.py:187
  225.6 15.1 %all-to-all-start.1 = ((bf16[128,24,2048]{2,1,0:T(8,128)(2,1)}), bf16[128,24,2048]{2,1,0:T(8,128)(2,1)}, u32[]{:S(2)}, u32[]{:S(2)}) async-start(bf16[128,24,2048]{2,1,0:T(8,128)(2,1)} %bitcast.94), calls=%async_computation.2 | async-start | bytes 25165824 | tf_op jit(solution)/shard_map/all_to_all | solution.py:190
  241.1 17.0 %all-gather.3.cloned.1.call-done = bf16[16384,256]{1,0:T(8,128)(2,1)} async-done(((bf16[128,256]{1,0:T(8,128)(2,1)}), bf16[16384,256]{1,0:T(8,128)(2,1)}) %all-gather.3.cloned.1.call-update) | async-done | bytes 8388624 | tf_op jit(solution)/shard_map/all_gather | solution.py:87
  258.2 57.2 %while.17 = (s32[]{:T(128)}, f32[4,512]{1,0:T(4,128)S(1)}, f32[4,512]{1,0:T(4,128)S(1)}, f32[4,512,64]{1,2,0:T(8,128)S(1)}, s32[32]{0:T(128)S(1)}, /*index=5*/s3...) while((s32[]{:T(128)}, f32[4,512]{1,0:T(4,128)S(1)}, ...), condition=%wide.region_7.8_spmd.clone, body=%wide.region_1.7_spmd.clone.sunk | while | flops 482656832 | bytes 25966364 | solution.py:134
  259.4 9.0 %conditional.3 = ((f32[4,512]{1,0:T(4,128)S(1)}, f32[4,512]{1,0:T(4,128)S(1)}, f32[4,512,64]{1,2,0:T(8,128)S(1)})) conditional(s32[]{:T(128)} %convert_element_type.193, (f32[4,512]{1,0:T(4,128)S(1)}, f32[4,512]{1,0:T(4,128)S(1)}, f32[4,512,64]{1,2,0:T(8,128)S(1)}) %tuple.59, (s32[]{:T(128)}, s32[512]{0:T(512)S(1)}, bf16[16384,256]{1,0:T(8,128)(2,1)}, ...), branch_computations={%region_2.2_spmd, %region_3.6_spmd} | conditional | flops 482649632 | bytes 25957090 | solution.py:129
  260.6 1.3 convolution_convert_fusion.1
  264.0 1.2 fusion.87
  266.0 1.3 convolution_convert_fusion
  269.6 9.0 %conditional.3 = ((f32[4,512]{1,0:T(4,128)S(1)}, f32[4,512]{1,0:T(4,128)S(1)}, f32[4,512,64]{1,2,0:T(8,128)S(1)})) conditional(s32[]{:T(128)} %convert_element_type.193, (f32[4,512]{1,0:T(4,128)S(1)}, f32[4,512]{1,0:T(4,128)S(1)}, f32[4,512,64]{1,2,0:T(8,128)S(1)}) %tuple.59, (s32[]{:T(128)}, s32[512]{0:T(512)S(1)}, bf16[16384,256]{1,0:T(8,128)(2,1)}, ...), branch_computations={%region_2.2_spmd, %region_3.6_spmd} | conditional | flops 482649632 | bytes 25957090 | solution.py:129
  270.7 1.3 convolution_convert_fusion.1
  274.2 1.2 fusion.87
  276.2 1.3 convolution_convert_fusion
  315.5 2.1 convolution_convert_fusion.4
  317.7 84.1 %all-to-all-done.1 = bf16[128,24,2048]{2,1,0:T(8,128)(2,1)} async-done(((bf16[128,24,2048]{2,1,0:T(8,128)(2,1)}), bf16[128,24,2048]{2,1,0:T(8,128)(2,1)}, u32[]{:S(2)}, u32[]{:S(2)}) %all-to-all-start.1) | async-done | bytes 12582944 | tf_op jit(solution)/shard_map/all_to_all | solution.py:190
  401.8 10.4 %bitcast_reduce_fusion = bf16[32,24,2048]{2,1,0:T(8,128)(2,1)} fusion(bf16[128,24,2048]{2,1,0:T(8,128)(2,1)} %all-to-all-done.1), kind=kLoop, calls=%fused_computation.62 | loop fusion | flops 4718592 | bytes 15728640 | tf_op jit(solution)/shard_map/reduce_sum | solution.py:199
  412.1 2.7 convolution_multiply_fusion.2
  416.3 1.6 fusion.45
  417.9 185.5 %reduce-scatter.2.cloned.1.call-done = bf16[128,2048]{1,0:T(8,128)(2,1)} async-done(((bf16[512,2048]{1,0:T(8,128)(2,1)}), bf16[128,2048]{1,0:T(8,128)(2,1)}) %reduce-scatter.2.cloned.1.call-update) | async-done | bytes 524304 | tf_op jit(solution)/shard_map/reduce_scatter | solution.py:148
  (283 shorter events, 38.5 us)
Async XLA Ops:
  7.2 199.4 %copy-start = (bf16[1,256,2048]{2,1,0:T(8,128)(2,1)S(1)}, bf16[1,256,2048]{2,1,0:T(8,128)(2,1)}, u32[]{:S(2)}) copy-start(bf16[1,256,2048]{2,1,0:T(8,128)(2,1)} %param.37) | copy-start | bytes 3145732
  7.2 233.9 %all-gather.5.cloned.1.call-start = ((), (), s32[]{:S(2)}) async-start(), calls=%async_computation.4 | async-start | bytes 1056768 | tf_op jit(solution)/shard_map/all_gather | solution.py:88
  7.9 250.1 %all-gather.3.cloned.1.call-start = ((), (), s32[]{:S(2)}) async-start(), calls=%async_computation.3 | async-start | bytes 8454144 | tf_op jit(solution)/shard_map/all_gather | solution.py:87
  25.5 12.0 %copy-start.6 = (bf16[128,512]{1,0:T(8,128)(2,1)S(1)}, bf16[128,512]{1,0:T(8,128)(2,1)}, u32[]{:S(2)}) copy-start(bf16[128,512]{1,0:T(8,128)(2,1)} %param.21) | copy-start | bytes 393220
  25.5 169.2 %copy-start.11 = (bf16[512,128]{1,0:T(8,128)(2,1)S(1)}, bf16[512,128]{1,0:T(8,128)(2,1)}, u32[]{:S(2)}) copy-start(bf16[512,128]{1,0:T(8,128)(2,1)} %param.27) | copy-start | bytes 393220
  25.5 169.2 %copy-start.12 = (f32[512]{0:T(512)S(1)}, f32[512]{0:T(512)}, u32[]{:S(2)}) copy-start(f32[512]{0:T(512)} %param.24) | copy-start | bytes 6148
  25.5 169.7 %copy-start.10 = (bf16[512,256]{1,0:T(8,128)(2,1)S(1)}, bf16[512,256]{1,0:T(8,128)(2,1)}, u32[]{:S(2)}) copy-start(bf16[512,256]{1,0:T(8,128)(2,1)} %param.26) | copy-start | bytes 786436
  25.5 171.4 %all-to-all-start = ((bf16[128,24,2048]{2,1,0:T(8,128)(2,1)}), bf16[128,24,2048]{2,1,0:T(8,128)(2,1)}, u32[]{:S(2)}, u32[]{:S(2)}) async-start(bf16[128,24,2048]{2,1,0:T(8,128)(2,1)} %bitcast.91), calls=%async_computation.1 | async-start | bytes 25165824 | tf_op jit(solution)/shard_map/all_to_all | solution.py:181
  37.4 159.5 %copy-start.9 = (bf16[1,2048,256]{2,1,0:T(8,128)(2,1)S(1)}, bf16[1,2048,256]{2,1,0:T(8,128)(2,1)}, u32[]{:S(2)}) copy-start(bf16[1,2048,256]{2,1,0:T(8,128)(2,1)} %param.35) | copy-start | bytes 3145732
  225.6 32.5 %copy-start.3 = (bf16[256,256]{1,0:T(8,128)(2,1)S(1)}, bf16[256,256]{1,0:T(8,128)(2,1)}, u32[]{:S(2)}) copy-start(bf16[256,256]{1,0:T(8,128)(2,1)} %param.28) | copy-start | bytes 393220
  225.6 32.5 %copy-start.4 = (bf16[256,256]{1,0:T(8,128)(2,1)S(1)}, bf16[256,256]{1,0:T(8,128)(2,1)}, u32[]{:S(2)}) copy-start(bf16[256,256]{1,0:T(8,128)(2,1)} %param.29) | copy-start | bytes 393220
  225.6 32.5 %copy-start.7 = (f32[256]{0:T(256)S(1)}, f32[256]{0:T(256)}, u32[]{:S(2)}) copy-start(f32[256]{0:T(256)} %param.25) | copy-start | bytes 3076
  225.6 176.1 %all-to-all-start.1 = ((bf16[128,24,2048]{2,1,0:T(8,128)(2,1)}), bf16[128,24,2048]{2,1,0:T(8,128)(2,1)}, u32[]{:S(2)}, u32[]{:S(2)}) async-start(bf16[128,24,2048]{2,1,0:T(8,128)(2,1)} %bitcast.94), calls=%async_computation.2 | async-start | bytes 25165824 | tf_op jit(solution)/shard_map/all_to_all | solution.py:190
  240.8 362.6 %reduce-scatter.2.cloned.1.call-start = ((), (), s32[]{:S(2)}) async-start(), calls=%async_computation.5 | async-start | bytes 2621440 | tf_op jit(solution)/shard_map/reduce_scatter | solution.py:148
  258.2 57.3 %copy-start.5 = (bf16[256,2048]{1,0:T(8,128)(2,1)S(1)}, bf16[256,2048]{1,0:T(8,128)(2,1)}, u32[]{:S(2)}) copy-start(bf16[256,2048]{1,0:T(8,128)(2,1)} %param.30) | copy-start | bytes 3145732
  315.4 2.2 copy-start.8
  412.1 2.8 copy-start.2
  415.6 187.8 %copy-start.1 = (bf16[1,256,2048]{2,1,0:T(8,128)(2,1)S(1)}, bf16[1,256,2048]{2,1,0:T(8,128)(2,1)}, u32[]{:S(2)}) copy-start(bf16[1,256,2048]{2,1,0:T(8,128)(2,1)} %param.37) | copy-start | bytes 3145732
Sparse Core Ops, SparseCore 0:
  10.8 144.9 all-gather.4
  159.0 99.0 all-gather.2
  317.8 285.5 reduce-scatter.1
where the time goes:
time: 616 us; the launch traced here: 610 us
  waiting for transfers between devices  289 us (47%)
  blocking collectives  157 us (25%)
  matrix products  52.5 us (9%)
  local copies, waits for them, and re-layouts  27.9 us (5%)
  starting transfers between devices  27.4 us (4%)
  other arithmetic  21.3 us (3%)
  loops' own time  20.8 us (3%)
  between operations  14 us (2%)
    reduce_scatter x1, waiting for transfers between devices, on_device(): lax.psum_scatter(lax.optimization_barrier(partial_out).astype(jnp.float32...  185 us
    all_gather x1, blocking collectives, on_device(): shard_rows = lax.all_gather(q_latent, 'tp', axis=0, tiled=True)  157 us
    all_to_all x1, waiting for transfers between devices, on_device(): lax.all_to_all(partial_out.reshape(sources, item_count, feature_width), (...  84.1 us
    another operation x1, loops' own time, on_device(): lax.scan(key_step, start_state, jnp.arange(shard_count // grouping, dtype...  20.2 us
    dot_general x1, matrix products, on_device(): jnp.dot(hidden, down_weight, preferred_element_type=jnp.float32)  19.1 us
    dynamic_slice x32, local copies, waits for them, and re-layouts, on_device(): lax.scan(key_step, start_state, jnp.arange(shard_count // grouping, dtype...  17.9 us
    all_gather x1, waiting for transfers between devices, on_device(): latents = lax.all_gather(kv_latent, ('ep', 'tp'), axis=0, tiled=True)  17 us
    all_to_all x1, starting transfers between devices, on_device(): lax.all_to_all(partial_out.reshape(sources, item_count, feature_width), (...  15.1 us
  transfers between devices with their start and end apart: 5, of which 4 were waited for; matrix products, arithmetic and copies ran while one was open for 17% of the time, Pallas kernels for 0%

commit v1 on v0

--- a/solution.py
+++ b/solution.py
@@ -63,7 +63,9 @@
     group_start = lax.axis_index("ep") * group_rows
     heads_here = w_key.shape[1] // NOPE
     score_scale = (NOPE + ROPE) ** (-0.5)
-    shard_rows = lax.all_gather(q_latent, "tp", axis=0, tiled=True)
+    shard_rows = jnp.concatenate(
+        lax.all_to_all(jnp.stack([q_latent] * lax.axis_size("tp")), "tp", 0, 0), axis=0
+    )
     row_count = shard_rows.shape[0]
     positions = group_start + jnp.arange(row_count, dtype=jnp.int32)
     cosine, sine_table = tables(positions)

time: 616 us -> 690 us (1.12)
  waiting for transfers between devices: 289 us -> 519 us
  blocking collectives: 157 us -> 0 us
    all_gather x1 -> x0, blocking collectives: 157 us -> none  [on_device(): shard_rows = lax.all_gather(q_latent, 'tp', axis=0, tiled=True)]
    all_to_all x1, waiting for transfers between devices: 1.2 us -> 157 us  [on_device(): lax.all_to_all(copies, ('ep', 'tp'), split_axis=0, concat_axis=0, tiled=T...]
    reduce_scatter x1, waiting for transfers between devices: 185 us -> 258 us  [on_device(): lax.psum_scatter(lax.optimization_barrier(partial_out).astype(jnp.float32...]
    all_gather x1, waiting for transfers between devices: 17 us -> 68.3 us  [on_device(): latents = lax.all_gather(kv_latent, ('ep', 'tp'), axis=0, tiled=True)]
    all_to_all x1, waiting for transfers between devices: 84.1 us -> 34.6 us  [on_device(): lax.all_to_all(partial_out.reshape(sources, item_count, feature_width), (...]
  transfers between devices with their start and end apart: 5 -> 6, of which waited for: 4 -> 4; matrix products, arithmetic and copies ran while one was open for 17% -> 15% of each run, Pallas kernels for 0% -> 0%
where the time goes in v1:
time: 690 us; the launch traced here: 684 us
  waiting for transfers between devices  519 us (75%)
  matrix products  52.3 us (8%)
  local copies, waits for them, and re-layouts  29.6 us (4%)
  starting transfers between devices  26.9 us (4%)
  other arithmetic  21.7 us (3%)
  loops' own time  20.8 us (3%)
  between operations  14 us (2%)
    reduce_scatter x1, waiting for transfers between devices, on_device(): lax.psum_scatter(lax.optimization_barrier(partial_out).astype(jnp.float32...  258 us
    all_to_all x1, waiting for transfers between devices, on_device(): lax.all_to_all(copies, ('ep', 'tp'), split_axis=0, concat_axis=0, tiled=T...  157 us
    all_gather x1, waiting for transfers between devices, on_device(): latents = lax.all_gather(kv_latent, ('ep', 'tp'), axis=0, tiled=True)  68.3 us
    all_to_all x1, waiting for transfers between devices, on_device(): lax.all_to_all(partial_out.reshape(sources, item_count, feature_width), (...  34.6 us
    another operation x1, loops' own time, on_device(): lax.scan(key_step, start_state, jnp.arange(shard_count // grouping, dtype...  20.1 us
    dot_general x1, matrix products, on_device(): jnp.dot(hidden, down_weight, preferred_element_type=jnp.float32)  18.8 us
    dynamic_slice x32, local copies, waits for them, and re-layouts, on_device(): lax.scan(key_step, start_state, jnp.arange(shard_count // grouping, dtype...  17.8 us
  transfers between devices with their start and end apart: 6, of which 4 were waited for; matrix products, arithmetic and copies ran while one was open for 15% of the time, Pallas kernels for 0%

profile of v1, /device:TPU:1, one launch (start us, length us, event | category | flops | bytes accessed | tf_op | source)
XLA Modules:
  0.0 684.0 jit_solution(611457448076789501)
XLA Ops:
  7.9 1.7 stack.2
  9.7 4.8 all-to-all-start
  19.9 3.9 convolution_convert_fusion.3
  23.8 8.2 %broadcast_in_dim.42 = bf16[32,4,24,2048]{3,2,1,0:T(8,128)(2,1)} broadcast(bf16[32,24,2048]{2,1,0:T(8,128)(2,1)} %bitcast.110), dimensions={0,2,3} | broadcast | bytes 15728640 | tf_op jit(solution)/shard_map/broadcast_in_dim | solution.py:179
  32.0 11.9 %all-to-all-start.1 = ((bf16[128,24,2048]{2,1,0:T(8,128)(2,1)}), bf16[128,24,2048]{2,1,0:T(8,128)(2,1)}, u32[]{:S(2)}, u32[]{:S(2)}) async-start(bf16[128,24,2048]{2,1,0:T(8,128)(2,1)} %bitcast.106), calls=%async_computation.2 | async-start | bytes 25165824 | tf_op jit(solution)/shard_map/all_to_all | solution.py:183
  45.6 156.7 %all-to-all-done.1 = bf16[128,24,2048]{2,1,0:T(8,128)(2,1)} async-done(((bf16[128,24,2048]{2,1,0:T(8,128)(2,1)}), bf16[128,24,2048]{2,1,0:T(8,128)(2,1)}, u32[]{:S(2)}, u32[]{:S(2)}) %all-to-all-start.1) | async-done | bytes 12582944 | tf_op jit(solution)/shard_map/all_to_all | solution.py:183
  202.3 10.0 %fusion.53 = f32[3072,256]{1,0:T(8,128)} fusion(bf16[3072,2048]{1,0:T(8,128)(2,1)} %bitcast.22, bf16[1,2048,256]{2,1,0:T(8,128)(2,1)} %param.35), kind=kOutput, calls=%fused_computation.85 | convolution fusion | flops 3221225472 | bytes 16777216 | tf_op jit(solution)/shard_map/dot_general | solution.py:186
  212.3 18.8 %convolution_convert_fusion.2 = bf16[3072,2048]{1,0:T(8,128)(2,1)} fusion(bf16[3072,2048]{1,0:T(8,128)(2,1)} %bitcast.22, f32[3072,256]{1,0:T(8,128)} %fusion.53, bf16[1,256,2048]{2,1,0:T(8,128)(2,1)S(1)} %copy-done, bf16[1,2048,256]{2,1,0:T(8,128)(2,1)S(1)} %copy-done.11), kind=kOutput, calls=%fused_computation.63 | convolution fusion | flops 6453460992 | bytes 30408704 | tf_op jit(solution)/shard_map/dot_general | solution.py:189
  231.1 9.9 %all-to-all-start.2 = ((bf16[128,24,2048]{2,1,0:T(8,128)(2,1)}), bf16[128,24,2048]{2,1,0:T(8,128)(2,1)}, u32[]{:S(2)}, u32[]{:S(2)}) async-start(bf16[128,24,2048]{2,1,0:T(8,128)(2,1)} %bitcast.109), calls=%async_computation.3 | async-start | bytes 25165824 | tf_op jit(solution)/shard_map/all_to_all | solution.py:192
  241.3 68.3 %all-gather.3.cloned.1.call-done = bf16[16384,256]{1,0:T(8,128)(2,1)} async-done(((bf16[128,256]{1,0:T(8,128)(2,1)}), bf16[16384,256]{1,0:T(8,128)(2,1)}) %all-gather.3.cloned.1.call-update) | async-done | bytes 8388624 | tf_op jit(solution)/shard_map/all_gather | solution.py:89
  309.7 57.2 %while.17 = (s32[]{:T(128)}, f32[4,512]{1,0:T(4,128)S(1)}, f32[4,512]{1,0:T(4,128)S(1)}, f32[4,512,64]{1,2,0:T(8,128)S(1)}, s32[32]{0:T(128)S(1)}, /*index=5*/s3...) while((s32[]{:T(128)}, f32[4,512]{1,0:T(4,128)S(1)}, ...), condition=%wide.region_7.8_spmd.clone, body=%wide.region_1.7_spmd.clone.sunk | while | flops 482656832 | bytes 25966364 | solution.py:136
  310.9 9.0 %conditional.3 = ((f32[4,512]{1,0:T(4,128)S(1)}, f32[4,512]{1,0:T(4,128)S(1)}, f32[4,512,64]{1,2,0:T(8,128)S(1)})) conditional(s32[]{:T(128)} %convert_element_type.202, (f32[4,512]{1,0:T(4,128)S(1)}, f32[4,512]{1,0:T(4,128)S(1)}, f32[4,512,64]{1,2,0:T(8,128)S(1)}) %tuple.60, (s32[]{:T(128)}, s32[512]{0:T(512)S(1)}, bf16[16384,256]{1,0:T(8,128)(2,1)}, ...), branch_computations={%region_2.2_spmd, %region_3.6_spmd} | conditional | flops 482649632 | bytes 25957090 | solution.py:131
  312.1 1.3 convolution_convert_fusion.1
  315.5 1.2 fusion.84
  317.6 1.3 convolution_convert_fusion
  321.1 9.0 %conditional.3 = ((f32[4,512]{1,0:T(4,128)S(1)}, f32[4,512]{1,0:T(4,128)S(1)}, f32[4,512,64]{1,2,0:T(8,128)S(1)})) conditional(s32[]{:T(128)} %convert_element_type.202, (f32[4,512]{1,0:T(4,128)S(1)}, f32[4,512]{1,0:T(4,128)S(1)}, f32[4,512,64]{1,2,0:T(8,128)S(1)}) %tuple.60, (s32[]{:T(128)}, s32[512]{0:T(512)S(1)}, bf16[16384,256]{1,0:T(8,128)(2,1)}, ...), branch_computations={%region_2.2_spmd, %region_3.6_spmd} | conditional | flops 482649632 | bytes 25957090 | solution.py:131
  322.3 1.3 convolution_convert_fusion.1
  327.7 1.3 convolution_convert_fusion
  367.0 2.1 convolution_convert_fusion.4
  369.1 34.6 %all-to-all-done.2 = bf16[128,24,2048]{2,1,0:T(8,128)(2,1)} async-done(((bf16[128,24,2048]{2,1,0:T(8,128)(2,1)}), bf16[128,24,2048]{2,1,0:T(8,128)(2,1)}, u32[]{:S(2)}, u32[]{:S(2)}) %all-to-all-start.2) | async-done | bytes 12582944 | tf_op jit(solution)/shard_map/all_to_all | solution.py:192
  403.7 10.4 %bitcast_reduce_fusion = bf16[32,24,2048]{2,1,0:T(8,128)(2,1)} fusion(bf16[128,24,2048]{2,1,0:T(8,128)(2,1)} %all-to-all-done.2), kind=kLoop, calls=%fused_computation.62 | loop fusion | flops 4718592 | bytes 15728640 | tf_op jit(solution)/shard_map/reduce_sum | solution.py:201
  414.0 2.7 convolution_multiply_fusion.2
  418.2 1.6 fusion.45
  419.8 257.6 %reduce-scatter.2.cloned.1.call-done = bf16[128,2048]{1,0:T(8,128)(2,1)} async-done(((bf16[512,2048]{1,0:T(8,128)(2,1)}), bf16[128,2048]{1,0:T(8,128)(2,1)}) %reduce-scatter.2.cloned.1.call-update) | async-done | bytes 524304 | tf_op jit(solution)/shard_map/reduce_scatter | solution.py:150
  (286 shorter events, 40.0 us)
Async XLA Ops:
  7.2 205.1 %copy-start = (bf16[1,256,2048]{2,1,0:T(8,128)(2,1)S(1)}, bf16[1,256,2048]{2,1,0:T(8,128)(2,1)}, u32[]{:S(2)}) copy-start(bf16[1,256,2048]{2,1,0:T(8,128)(2,1)} %param.37) | copy-start | bytes 3145732
  7.2 234.1 %all-gather.5.cloned.1.call-start = ((), (), s32[]{:S(2)}) async-start(), calls=%async_computation.5 | async-start | bytes 1056768 | tf_op jit(solution)/shard_map/all_gather | solution.py:90
  9.7 14.2 %all-to-all-start = ((bf16[4,128,512]{2,1,0:T(8,128)(2,1)}), bf16[4,128,512]{2,1,0:T(8,128)(2,1)S(1)}, u32[]{:S(2)}, u32[]{:S(2)}) async-start(bf16[4,128,512]{2,1,0:T(8,128)(2,1)} %stack.2), calls=%async_computation | async-start | bytes 1048576 | tf_op jit(solution)/shard_map/all_to_all | solution.py:67
  14.5 295.1 %all-gather.3.cloned.1.call-start = ((), (), s32[]{:S(2)}) async-start(), calls=%async_computation.4 | async-start | bytes 8454144 | tf_op jit(solution)/shard_map/all_gather | solution.py:89
  32.0 11.9 %copy-start.7 = (bf16[512,128]{1,0:T(8,128)(2,1)S(1)}, bf16[512,128]{1,0:T(8,128)(2,1)}, u32[]{:S(2)}) copy-start(bf16[512,128]{1,0:T(8,128)(2,1)} %param.27) | copy-start | bytes 393220
  32.0 12.4 %copy-start.9 = (f32[512]{0:T(512)S(1)}, f32[512]{0:T(512)}, u32[]{:S(2)}) copy-start(f32[512]{0:T(512)} %param.24) | copy-start | bytes 6148
  32.0 170.3 %all-to-all-start.1 = ((bf16[128,24,2048]{2,1,0:T(8,128)(2,1)}), bf16[128,24,2048]{2,1,0:T(8,128)(2,1)}, u32[]{:S(2)}, u32[]{:S(2)}) async-start(bf16[128,24,2048]{2,1,0:T(8,128)(2,1)} %bitcast.106), calls=%async_computation.2 | async-start | bytes 25165824 | tf_op jit(solution)/shard_map/all_to_all | solution.py:183
  43.9 1.3 copy-start.6
  202.3 10.0 %copy-start.11 = (bf16[1,2048,256]{2,1,0:T(8,128)(2,1)S(1)}, bf16[1,2048,256]{2,1,0:T(8,128)(2,1)}, u32[]{:S(2)}) copy-start(bf16[1,2048,256]{2,1,0:T(8,128)(2,1)} %param.36) | copy-start | bytes 3145732
  231.1 78.6 %copy-start.3 = (bf16[256,256]{1,0:T(8,128)(2,1)S(1)}, bf16[256,256]{1,0:T(8,128)(2,1)}, u32[]{:S(2)}) copy-start(bf16[256,256]{1,0:T(8,128)(2,1)} %param.28) | copy-start | bytes 393220
  231.1 78.6 %copy-start.4 = (bf16[256,256]{1,0:T(8,128)(2,1)S(1)}, bf16[256,256]{1,0:T(8,128)(2,1)}, u32[]{:S(2)}) copy-start(bf16[256,256]{1,0:T(8,128)(2,1)} %param.29) | copy-start | bytes 393220
  231.1 78.6 %copy-start.8 = (f32[256]{0:T(256)S(1)}, f32[256]{0:T(256)}, u32[]{:S(2)}) copy-start(f32[256]{0:T(256)} %param.25) | copy-start | bytes 3076
  231.1 172.6 %all-to-all-start.2 = ((bf16[128,24,2048]{2,1,0:T(8,128)(2,1)}), bf16[128,24,2048]{2,1,0:T(8,128)(2,1)}, u32[]{:S(2)}, u32[]{:S(2)}) async-start(bf16[128,24,2048]{2,1,0:T(8,128)(2,1)} %bitcast.109), calls=%async_computation.3 | async-start | bytes 25165824 | tf_op jit(solution)/shard_map/all_to_all | solution.py:192
  241.0 436.5 %reduce-scatter.2.cloned.1.call-start = ((), (), s32[]{:S(2)}) async-start(), calls=%async_computation.6 | async-start | bytes 2621440 | tf_op jit(solution)/shard_map/reduce_scatter | solution.py:150
  309.7 57.2 %copy-start.5 = (bf16[256,2048]{1,0:T(8,128)(2,1)S(1)}, bf16[256,2048]{1,0:T(8,128)(2,1)}, u32[]{:S(2)}) copy-start(bf16[256,2048]{1,0:T(8,128)(2,1)} %param.30) | copy-start | bytes 3145732
  366.9 2.2 copy-start.10
  414.0 2.8 copy-start.2
  417.5 259.9 %copy-start.1 = (bf16[1,256,2048]{2,1,0:T(8,128)(2,1)S(1)}, bf16[1,256,2048]{2,1,0:T(8,128)(2,1)}, u32[]{:S(2)}) copy-start(bf16[1,256,2048]{2,1,0:T(8,128)(2,1)} %param.37) | copy-start | bytes 3145732
Sparse Core Ops, SparseCore 0:
  10.8 147.3 all-gather.4
  161.3 148.2 all-gather.2
  369.2 308.1 reduce-scatter.1
